TPU v7x, 32 devices: a whole 2x2x4 slice. The times are simulated.
32 devices in a mesh: row: 16 (over z, y, x), col: 2 (over core).
Axes of the slice: x: 2, y: 2, z: 4, core: 2. Of those that a mesh axis runs over, the one named last changes fastest.
Arguments:
- tokens: bfloat16 [2, 3072, 2048], P('col', 'row'), may hold values from -6 to 6
- proj_in: bfloat16 [2048, 512], P('col'), may hold values from -0.125 to 0.125
- proj_out: bfloat16 [512, 2048], P(None, 'row'), may hold values from -0.25 to 0.25
Outputs:
- output: bfloat16 [2, 3072, 2048], P('col', 'row')
All inputs are finite; a program needn't handle non-finite values.
Results may differ from a plain program's by a relative error of at most 0.0083.
Values may be sent and summed in bfloat16 or wider, within the bound.
A program may use at most 64 MiB of HBM per device.

v0:
```python
import math
import jax
import jax.numpy as jnp
from jax import lax
from jax.sharding import PartitionSpec as P

GRP = 128
highest = lax.Precision.HIGHEST
span_inner = 128


def circle(height, breadth, period):
    product = lax.iota(jnp.int32, height)[:, None] * lax.iota(jnp.int32, breadth)[None, :] % period
    angle = product.astype(jnp.float32) * (2.0 * math.pi / period)
    return (jnp.cos(angle), jnp.sin(angle))


def positions(piece):
    real_in = piece[0, 0]
    imag_in = piece[1, 0]
    count, length = real_in.shape
    outer = length // span_inner
    real_in = real_in.reshape(count, outer, span_inner)
    imag_in = imag_in.reshape(count, outer, span_inner)
    cos_one, sin_one = circle(outer, outer, outer)
    first_re = jnp.einsum("ab,kbq->kaq", cos_one, real_in, precision=highest) - jnp.einsum(
        "ab,kbq->kaq", sin_one, imag_in, precision=highest
    )
    first_im = jnp.einsum("ab,kbq->kaq", sin_one, real_in, precision=highest) + jnp.einsum(
        "ab,kbq->kaq", cos_one, imag_in, precision=highest
    )
    twist_c, twist_s = circle(outer, span_inner, length)
    turned_re = first_re * twist_c - first_im * twist_s
    turned_im = first_re * twist_s + first_im * twist_c
    cos_two, sin_two = circle(span_inner, span_inner, span_inner)
    factor = 1.0 / math.sqrt(GRP * length)
    real_out = jnp.einsum("kaq,qb->kba", turned_re, cos_two, precision=highest) - jnp.einsum(
        "kaq,qb->kba", turned_im, sin_two, precision=highest
    )
    real_out = real_out.reshape(count, length) * factor
    return real_out[:, None, :]


def shards(tokens, proj_in, proj_out):
    seq_rows = tokens[0]
    local_len = seq_rows.shape[0]
    features = proj_in.shape[1]
    groups = features // GRP
    mapped = jnp.dot(
        seq_rows,
        lax.all_gather(proj_in, "col", axis=0, tiled=True),
        preferred_element_type=jnp.float32,
    ).astype(jnp.bfloat16)
    values = mapped.astype(jnp.float32).reshape(local_len, groups, GRP)
    cos_c, sin_c = circle(GRP, GRP, GRP)
    real_part = jnp.einsum("pgc,cs->gsp", values, cos_c, precision=highest)
    imag_part = jnp.einsum("pgc,cs->gsp", values, sin_c, precision=highest)
    ways = lax.axis_size("row")
    slots = groups * cos_c.shape[1]
    per_dev = slots // ways
    stacked = jnp.stack(
        [real_part.reshape(ways, per_dev, local_len), imag_part.reshape(ways, per_dev, local_len)],
        0,
    )
    spectra = positions(lax.all_to_all(stacked, "row", split_axis=1, concat_axis=3, tiled=True))
    outgoing = spectra.astype(jnp.bfloat16)
    back = lax.all_to_all(outgoing, "row", split_axis=2, concat_axis=0, tiled=True)
    mixed = back.reshape(features, local_len)
    result = lax.dot_general(
        mixed,
        lax.all_gather(proj_out, "row", axis=1, tiled=True),
        (((0,), (0,)), ((), ())),
        preferred_element_type=jnp.float32,
    )
    return result.astype(jnp.bfloat16)[None]


def solution(mesh):
    in_specs = (P("col", "row", None), P("col", None), P(None, "row"))
    out_specs = P("col", "row", None)
    return jax.shard_map(shards, mesh=mesh, in_specs=in_specs, out_specs=out_specs, check_vma=False)
```

profile of v0, /device:TPU:0, one launch (start us, length us, event | category | flops | bytes accessed | tf_op | source)
XLA Modules:
  0.0 115.2 jit_solution(4672272364211628046)
XLA Ops:
  6.5 0.0 copy-start
  6.5 0.0 all-gather.3.cloned.1.call-start
  6.5 0.7 all-gather.3.cloned.1.call-update
  7.3 0.0 all-gather.5.cloned.1.call-start
  7.3 0.7 all-gather.5.cloned.1.call-update
  8.0 14.2 %all-gather.3.cloned.1.call-done = bf16[2048,512]{1,0:T(8,128)(2,1)} async-done(((bf16[1024,512]{1,0:T(8,128)(2,1)}), bf16[2048,512]{1,0:T(8,128)(2,1)}) %all-gather.3.cloned.1.call-update) | async-done | bytes 2097168 | tf_op jit(solution)/shard_map/all_gather | solution.py:51
  22.2 0.0 copy-done
  22.2 2.2 %fusion.5 = bf16[24,4,8,128]{3,2,1,0:T(8,128)(2,1)S(1)} fusion(bf16[2048,512]{1,0:T(8,128)(2,1)} %all-gather.3.cloned.1.call-done, bf16[1,192,2048]{2,1,0:T(8,128)(2,1)S(1)} %copy-done), kind=kOutput, calls=%fused_computation.12 | convolution fusion | flops 402751488 | bytes 3080192 | tf_op jit(solution)/shard_map/dot_general | solution.py:49
  24.4 0.6 convolution_bitcast_fusion.1
  24.9 0.2 copy.19
  25.2 0.6 convolution_bitcast_fusion
  25.7 0.2 copy.21
  25.9 0.1 pad_maximum_fusion
  26.0 1.1 copy.22
  27.1 6.8 %all-to-all-start = ((f32[2,16,32,192]{3,2,0,1:T(8,128)}), f32[2,16,32,192]{3,2,0,1:T(8,128)S(1)}, u32[]{:S(2)}, u32[]{:S(2)}) async-start(f32[2,16,32,192]{3,2,0,1:T(8,128)} %copy.22), calls=%async_computation | async-start | bytes 2097152 | tf_op jit(solution)/shard_map/all_to_all | solution.py:65
  33.9 0.1 fusion.43
  34.0 24.7 %all-to-all-done = f32[2,16,32,192]{3,2,0,1:T(8,128)S(1)} async-done(((f32[2,16,32,192]{3,2,0,1:T(8,128)}), f32[2,16,32,192]{3,2,0,1:T(8,128)S(1)}, u32[]{:S(2)}, u32[]{:S(2)}) %all-to-all-start) | async-done | bytes 786464 | tf_op jit(solution)/shard_map/all_to_all | solution.py:65
  58.7 0.1 fusion.95
  58.8 0.3 copy.23
  59.1 0.3 reshape_squeeze.6
  59.4 0.3 copy.24
  59.7 0.3 reshape_squeeze.7
  60.0 0.5 fusion.39
  60.5 0.5 fusion.35
  61.0 0.5 fusion.2
  61.6 0.6 multiply_add_fusion
  62.2 0.7 fusion.9
  62.9 0.7 fusion.6
  63.7 0.4 copy.31
  64.1 0.4 reshape.66
  64.5 0.5 broadcast.106
  65.0 17.0 %reduce = bf16[3072,32]{1,0:T(8,128)(2,1)S(1)} reduce(bf16[3072,1,32]{2,1,0:T(2,128)(2,1)S(1)} %bitcast.68, bf16[]{:T(256)} %broadcast.106), dimensions={1}, to_apply=%bitcast.57.reduce_sub_computation | reduce | bytes 393218
  82.0 0.8 reshape.67
  82.7 19.8 %all_to_all.30 = bf16[16,2,3072]{2,1,0:T(2,128)(2,1)S(1)} all-to-all(bf16[16,2,3072]{2,1,0:T(2,128)(2,1)S(1)} %reshape.67), channel_id=1, replica_groups=mesh['row'=16,'col'=2] {'row'}, dimensions={0} | all-to-all | bytes 393216 | tf_op jit(solution)/shard_map/all_to_all | solution.py:67
  102.6 0.9 reshape.68
  103.4 1.4 %copy.29 = bf16[32,1,3072]{2,0,1:T(8,128)(2,1)S(1)} copy(bf16[32,1,3072]{0,1,2:T(2,128)(2,1)S(1)} %bitcast.69) | data formatting | bytes 393216 | tf_op jit(solution)/shard_map/all_to_all | solution.py:67
  104.8 0.3 all_to_all.26
  105.1 0.1 copy.30
  105.2 0.0 all-gather.5.cloned.1.call-done
  105.2 3.1 %fusion = bf16[1,192,2048]{2,1,0:T(8,128)(2,1)} fusion(bf16[512,192]{1,0:T(8,128)(2,1)S(1)} %bitcast.73, bf16[512,2048]{1,0:T(8,128)(2,1)} %all-gather.5.cloned.1.call-done), kind=kOutput, calls=%fused_computation.1 | convolution fusion | flops 403046400 | bytes 3080192 | tf_op jit(solution)/shard_map/dot_general | solution.py:69
Async XLA Ops:
  6.5 15.7 %copy-start = (bf16[1,192,2048]{2,1,0:T(8,128)(2,1)S(1)}, bf16[1,192,2048]{2,1,0:T(8,128)(2,1)}, u32[]{:S(2)}) copy-start(bf16[1,192,2048]{2,1,0:T(8,128)(2,1)} %param.3) | copy-start | bytes 2359300
  6.5 15.7 %all-gather.3.cloned.1.call-start = ((), (), s32[]{:S(2)}) async-start(), calls=%async_computation.2 | async-start | bytes 3145728 | tf_op jit(solution)/shard_map/all_gather | solution.py:51
  7.3 98.0 %all-gather.5.cloned.1.call-start = ((), (), s32[]{:S(2)}) async-start(), calls=%async_computation.3 | async-start | bytes 2228224 | tf_op jit(solution)/shard_map/all_gather | solution.py:71
  27.1 31.6 %all-to-all-start = ((f32[2,16,32,192]{3,2,0,1:T(8,128)}), f32[2,16,32,192]{3,2,0,1:T(8,128)S(1)}, u32[]{:S(2)}, u32[]{:S(2)}) async-start(f32[2,16,32,192]{3,2,0,1:T(8,128)} %copy.22), calls=%async_computation | async-start | bytes 2097152 | tf_op jit(solution)/shard_map/all_to_all | solution.py:65
Sparse Core Ops, SparseCore 0:
  8.9 13.2 all-gather.2
  24.9 73.4 all-gather.4
where the time goes:
time: 115 us
  waiting for transfers between devices  40.3 us (35%)
  blocking collectives  19.8 us (17%)
  other arithmetic  17.1 us (15%)
  between operations  13.6 us (12%)
  matrix products  10 us (9%)
  local copies, waits for them, and re-layouts  7.43 us (6%)
  starting transfers between devices  6.84 us (6%)
    all_to_all x1, waiting for transfers between devices, shards(): lax.all_to_all(stacked, 'row', split_axis=1, concat_axis=3, tiled=True)  24.7 us
    all_to_all x1, blocking collectives, shards(): lax.all_to_all(outgoing, 'row', split_axis=2, concat_axis=0, tiled=True)  19.8 us
    unnamed x1, other arithmetic  17 us
    all_gather x1, waiting for transfers between devices, shards(): lax.all_gather(proj_in, 'col', axis=0, tiled=True)  14.2 us
    all_to_all x1, starting transfers between devices, shards(): lax.all_to_all(stacked, 'row', split_axis=1, concat_axis=3, tiled=True)  6.8 us
    dot_general x1, matrix products, shards(): lax.dot_general(mixed, lax.all_gather(proj_out, 'row', axis=1, tiled=True...  3.08 us
  transfers between devices with their start and end apart: 3, of which 2 were waited for; matrix products, arithmetic and copies ran while one was open for 27% of the time, Pallas kernels for 0%

commit v1 on v0

--- a/solution.py
+++ b/solution.py
@@ -62,7 +62,14 @@
         [real_part.reshape(ways, per_dev, local_len), imag_part.reshape(ways, per_dev, local_len)],
         0,
     )
-    spectra = positions(lax.all_to_all(stacked, "row", split_axis=1, concat_axis=3, tiled=True))
+    spectra = positions(
+        jnp.concatenate(
+            lax.all_to_all(
+                jnp.stack(jnp.split(stacked, lax.axis_size("row"), axis=1)), "row", 0, 0
+            ),
+            axis=3,
+        )
+    )
     outgoing = spectra.astype(jnp.bfloat16)
     back = lax.all_to_all(outgoing, "row", split_axis=2, concat_axis=0, tiled=True)
     mixed = back.reshape(features, local_len)

time: 115 us -> 127 us (1.10)
  other arithmetic: 17.1 us -> 27 us
  waiting for transfers between devices: 40.3 us -> 48.6 us
  blocking collectives: 19.8 us -> 13.9 us
    unnamed x1 -> x16, other arithmetic: 17 us -> 26.4 us
    all_to_all x1, waiting for transfers between devices: 24.7 us -> 33 us  [shards(): lax.all_to_all(jnp.stack(jnp.split(stacked, lax.axis_size('row'), axis=1)...]
    all_to_all x1, blocking collectives: 19.8 us -> 13.9 us  [shards(): lax.all_to_all(outgoing, 'row', split_axis=2, concat_axis=0, tiled=True)]
  transfers between devices with their start and end apart: 3 -> 3, of which waited for: 2 -> 2; matrix products, arithmetic and copies ran while one was open for 27% -> 32% of each run, Pallas kernels for 0% -> 0%
where the time goes in v1:
time: 127 us; the launch traced here: 126 us
  waiting for transfers between devices  48.6 us (38%)
  other arithmetic  27 us (21%)
  blocking collectives  13.9 us (11%)
  between operations  13.6 us (11%)
  matrix products  10 us (8%)
  starting transfers between devices  6.84 us (5%)
  local copies, waits for them, and re-layouts  6.34 us (5%)
    all_to_all x1, waiting for transfers between devices, shards(): lax.all_to_all(jnp.stack(jnp.split(stacked, lax.axis_size('row'), axis=1)...  33 us
    unnamed x16, other arithmetic  26.4 us
    all_gather x1, waiting for transfers between devices, shards(): lax.all_gather(proj_in, 'col', axis=0, tiled=True)  14.2 us
    all_to_all x1, blocking collectives, shards(): lax.all_to_all(outgoing, 'row', split_axis=2, concat_axis=0, tiled=True)  13.9 us
    all_to_all x1, starting transfers between devices, shards(): lax.all_to_all(jnp.stack(jnp.split(stacked, lax.axis_size('row'), axis=1)...  6.8 us
    dot_general x1, matrix products, shards(): lax.dot_general(mixed, lax.all_gather(proj_out, 'row', axis=1, tiled=True...  3.08 us
  transfers between devices with their start and end apart: 3, of which 2 were waited for; matrix products, arithmetic and copies ran while one was open for 32% of the time, Pallas kernels for 0%

profile of v1, /device:TPU:0, one launch (start us, length us, event | category | flops | bytes accessed | tf_op | source)
XLA Modules:
  0.0 126.4 jit_solution(7654711350104280932)
XLA Ops:
  6.5 0.0 copy-start
  6.5 0.0 all-gather.3.cloned.1.call-start
  6.5 0.7 all-gather.3.cloned.1.call-update
  7.3 0.0 all-gather.5.cloned.1.call-start
  7.3 0.7 all-gather.5.cloned.1.call-update
  8.0 14.2 %all-gather.3.cloned.1.call-done = bf16[2048,512]{1,0:T(8,128)(2,1)} async-done(((bf16[1024,512]{1,0:T(8,128)(2,1)}), bf16[2048,512]{1,0:T(8,128)(2,1)}) %all-gather.3.cloned.1.call-update) | async-done | bytes 2097168 | tf_op jit(solution)/shard_map/all_gather | solution.py:51
  22.2 0.0 copy-done
  22.2 2.2 %fusion.5 = bf16[24,4,8,128]{3,2,1,0:T(8,128)(2,1)S(1)} fusion(bf16[2048,512]{1,0:T(8,128)(2,1)} %all-gather.3.cloned.1.call-done, bf16[1,192,2048]{2,1,0:T(8,128)(2,1)S(1)} %copy-done), kind=kOutput, calls=%fused_computation.42 | convolution fusion | flops 402751488 | bytes 3080192 | tf_op jit(solution)/shard_map/dot_general | solution.py:49
  24.4 0.6 convolution_bitcast_fusion.1
  24.9 0.6 convolution_bitcast_fusion
  25.5 0.2 copy.49
  25.7 0.2 copy.51
  25.9 0.6 bitcast_dynamic-update-slice_fusion.14
  26.6 0.6 bitcast_dynamic-update-slice_fusion.13
  27.2 0.6 bitcast_dynamic-update-slice_fusion.12
  27.8 0.6 bitcast_dynamic-update-slice_fusion.11
  28.4 0.6 bitcast_dynamic-update-slice_fusion.10
  29.1 0.6 bitcast_dynamic-update-slice_fusion.9
  29.7 0.6 bitcast_dynamic-update-slice_fusion.8
  30.3 0.6 bitcast_dynamic-update-slice_fusion.7
  30.9 0.6 bitcast_dynamic-update-slice_fusion.6
  31.6 0.6 bitcast_dynamic-update-slice_fusion.5
  32.2 0.6 bitcast_dynamic-update-slice_fusion.4
  32.8 0.6 bitcast_dynamic-update-slice_fusion.3
  33.4 0.6 bitcast_dynamic-update-slice_fusion.2
  34.1 0.6 bitcast_dynamic-update-slice_fusion.1
  34.7 0.6 bitcast_dynamic-update-slice_fusion
  35.3 0.6 fusion.34
  35.9 6.8 %all-to-all-start = ((f32[16,2,1,32,192]{4,3,1,2,0:T(8,128)}), f32[16,2,1,32,192]{4,3,1,2,0:T(8,128)S(1)}, u32[]{:S(2)}, u32[]{:S(2)}) async-start(f32[16,2,1,32,192]{4,3,1,2,0:T(8,128)} %fusion.34), calls=%async_computation | async-start | bytes 2097152 | tf_op jit(solution)/shard_map/all_to_all | solution.py:67
  42.7 0.1 fusion.60
  42.8 33.0 %all-to-all-done = f32[16,2,1,32,192]{4,3,1,2,0:T(8,128)S(1)} async-done(((f32[16,2,1,32,192]{4,3,1,2,0:T(8,128)}), f32[16,2,1,32,192]{4,3,1,2,0:T(8,128)S(1)}, u32[]{:S(2)}, u32[]{:S(2)}) %all-to-all-start) | async-done | bytes 786464 | tf_op jit(solution)/shard_map/all_to_all | solution.py:67
  75.8 0.1 fusion.112
  75.9 0.3 copy.67
  76.2 0.3 reshape_squeeze.6
  76.5 0.3 copy.68
  76.9 0.3 reshape_squeeze.7
  77.1 0.5 fusion.56
  77.7 0.5 fusion.52
  78.2 0.5 fusion.2
  78.7 0.6 multiply_add_fusion
  79.3 0.7 fusion.9
  80.1 0.7 fusion.6
  80.8 0.4 copy.75
  81.3 0.4 reshape.71
  81.6 0.5 broadcast.106
  82.2 17.0 %reduce = bf16[3072,32]{1,0:T(8,128)(2,1)S(1)} reduce(bf16[3072,1,32]{2,1,0:T(2,128)(2,1)S(1)} %bitcast.162, bf16[]{:T(256)} %broadcast.106), dimensions={1}, to_apply=%bitcast.119.reduce_sub_computation | reduce | bytes 393218
  99.1 0.8 reshape.72
  99.9 13.9 %all_to_all.20 = bf16[16,2,3072]{2,1,0:T(2,128)(2,1)S(1)} all-to-all(bf16[16,2,3072]{2,1,0:T(2,128)(2,1)S(1)} %reshape.72), channel_id=1, replica_groups=mesh['row'=16,'col'=2] {'row'}, dimensions={0} | all-to-all | bytes 393216 | tf_op jit(solution)/shard_map/all_to_all | solution.py:74
  113.8 0.9 reshape.73
  114.7 1.4 %copy.73 = bf16[32,1,3072]{2,0,1:T(8,128)(2,1)S(1)} copy(bf16[32,1,3072]{0,1,2:T(2,128)(2,1)S(1)} %bitcast.163) | data formatting | bytes 393216 | tf_op jit(solution)/shard_map/all_to_all | solution.py:74
  116.1 0.3 all_to_all.16
  116.4 0.1 copy.74
  116.5 0.0 all-gather.5.cloned.1.call-done
  116.5 3.1 %fusion = bf16[1,192,2048]{2,1,0:T(8,128)(2,1)} fusion(bf16[512,192]{1,0:T(8,128)(2,1)S(1)} %bitcast.165, bf16[512,2048]{1,0:T(8,128)(2,1)} %all-gather.5.cloned.1.call-done), kind=kOutput, calls=%fused_computation.31 | convolution fusion | flops 403046400 | bytes 3080192 | tf_op jit(solution)/shard_map/dot_general | solution.py:76
Async XLA Ops:
  6.5 15.7 %copy-start = (bf16[1,192,2048]{2,1,0:T(8,128)(2,1)S(1)}, bf16[1,192,2048]{2,1,0:T(8,128)(2,1)}, u32[]{:S(2)}) copy-start(bf16[1,192,2048]{2,1,0:T(8,128)(2,1)} %param.3) | copy-start | bytes 2359300
  6.5 15.7 %all-gather.3.cloned.1.call-start = ((), (), s32[]{:S(2)}) async-start(), calls=%async_computation.2 | async-start | bytes 3145728 | tf_op jit(solution)/shard_map/all_gather | solution.py:51
  7.3 109.2 %all-gather.5.cloned.1.call-start = ((), (), s32[]{:S(2)}) async-start(), calls=%async_computation.3 | async-start | bytes 2228224 | tf_op jit(solution)/shard_map/all_gather | solution.py:78
  35.9 39.9 %all-to-all-start = ((f32[16,2,1,32,192]{4,3,1,2,0:T(8,128)}), f32[16,2,1,32,192]{4,3,1,2,0:T(8,128)S(1)}, u32[]{:S(2)}, u32[]{:S(2)}) async-start(f32[16,2,1,32,192]{4,3,1,2,0:T(8,128)} %fusion.34), calls=%async_computation | async-start | bytes 2097152 | tf_op jit(solution)/shard_map/all_to_all | solution.py:67
Sparse Core Ops, SparseCore 0:
  8.9 13.2 all-gather.2
  24.9 74.8 all-gather.4
